TPU v7x, 32 devices: a whole 2x2x4 slice. The times are simulated.
32 devices in a mesh: ra: 8 (over z, y), cb: 4 (over x, core).
Axes of the slice: x: 2, y: 2, z: 4, core: 2. Of those that a mesh axis runs over, the one named last changes fastest.
Arguments:
- tokens: bfloat16 [512, 4096], P(None, 'ra'), may hold values from -4 to 4, as said below
- pre_gain_first: float32 [4096], P('ra'), may hold values from 0.1 to 1.9
- gate_first: bfloat16 [4096, 11264], P('ra', 'cb'), may hold values from -0.125 to 0.125
- up_first: bfloat16 [4096, 11264], P('ra', 'cb'), may hold values from -0.125 to 0.125
- down_first: bfloat16 [11264, 4096], P('cb', 'ra'), may hold values from -0.078125 to 0.078125
- post_gain_first: float32 [4096], P('ra'), may hold values from 0.1 to 1.9
- pre_gain_second: float32 [4096], P('ra'), may hold values from 0.1 to 1.9
- gate_second: bfloat16 [4096, 11264], P('ra', 'cb'), may hold values from -0.125 to 0.125
- up_second: bfloat16 [4096, 11264], P('ra', 'cb'), may hold values from -0.125 to 0.125
- down_second: bfloat16 [11264, 4096], P('cb', 'ra'), may hold values from -0.078125 to 0.078125
- post_gain_second: float32 [4096], P('ra'), may hold values from 0.1 to 1.9
Outputs:
- mixed: bfloat16 [512, 4096], P(None, 'ra')
Inputs may be any that keep to these rules, and one draw needn't show every extreme that they name: `tokens`: each block of 128 consecutive channels has its own scale, and rows have their own scales.
All inputs are finite; a program needn't handle non-finite values.
Results may differ from a plain program's by a relative error of at most 0.0071.
Values may be sent and summed in bfloat16 or wider, within the bound.
A program may use at most 64 MiB of HBM per device.

v0:
```python
import jax
import jax.numpy as jnp
from jax import lax
from jax.sharding import PartitionSpec as P

D = 4096


EPS = 1e-06


def row_scale(sum_squares):
    return lax.rsqrt(sum_squares / D + EPS)


def branch_value(resid, scale, pre_gain, gate_weight, up_weight, down_weight):
    normed = (resid * scale[:, None] * pre_gain[None, :]).astype(jnp.bfloat16)
    gate_value = jnp.dot(normed, gate_weight, preferred_element_type=jnp.float32)
    up_value = jnp.dot(normed, up_weight, preferred_element_type=jnp.float32)
    gate_value, up_value = (
        lax.psum_scatter(gate_value, "ra", scatter_dimension=0, tiled=True),
        lax.psum_scatter(up_value, "ra", scatter_dimension=0, tiled=True),
    )
    hidden = (jax.nn.silu(gate_value) * up_value).astype(jnp.bfloat16)
    partial_out = jnp.dot(
        lax.all_gather(hidden, "ra", axis=0, tiled=True),
        down_weight,
        preferred_element_type=jnp.float32,
    )
    return lax.psum(partial_out, "cb")


def body(
    tokens,
    pre_gain_first,
    gate_first,
    up_first,
    down_first,
    post_gain_first,
    pre_gain_second,
    gate_second,
    up_second,
    down_second,
    post_gain_second,
):
    resid = tokens.astype(jnp.float32)
    input_total = lax.psum(jnp.sum(resid * resid, axis=1), "ra")
    branch_first = branch_value(
        resid, row_scale(input_total), pre_gain_first, gate_first, up_first, down_first
    )
    first_total = lax.psum(jnp.sum(branch_first * branch_first, axis=1), "ra")
    factor = 0.5 * row_scale(first_total)
    middle = resid + factor[:, None] * branch_first * post_gain_first[None, :]
    middle_total = lax.psum(jnp.sum(middle * middle, axis=1), "ra")
    branch_second = branch_value(
        middle, row_scale(middle_total), pre_gain_second, gate_second, up_second, down_second
    )
    second_total = lax.psum(jnp.sum(branch_second * branch_second, axis=1), "ra")
    final = (
        middle + 0.5 * row_scale(second_total)[:, None] * branch_second * post_gain_second[None, :]
    )
    return final.astype(jnp.bfloat16)


def solution(mesh):
    in_specs = (
        P(None, "ra"),
        P("ra"),
        P("ra", "cb"),
        P("ra", "cb"),
        P("cb", "ra"),
        P("ra"),
        P("ra"),
        P("ra", "cb"),
        P("ra", "cb"),
        P("cb", "ra"),
        P("ra"),
    )
    out_specs = P(None, "ra")
    return jax.shard_map(body, mesh=mesh, in_specs=in_specs, out_specs=out_specs, check_vma=False)
```

profile of v0, /device:TPU:0, one launch (start us, length us, event | category | flops | bytes accessed | tf_op | source)
XLA Modules:
  0.0 760.4 jit_solution(3636194673034260078)
XLA Ops:
  6.5 0.0 copy-start
  6.5 0.0 reduce-scatter.7.cloned.1.call-start
  6.5 1.4 fusion
  7.9 23.2 %psum.42 = f32[512]{0:T(512)S(1)} all-reduce(f32[512]{0:T(512)S(1)} %fusion), channel_id=1, replica_groups=mesh['ra'=8,'cb'=4] {'ra'}, use_global_device_ids=true, to_apply=%region_1.0 | all-reduce | flops 512 | bytes 4096 | tf_op jit(solution)/shard_map/psum | solution.py:47
  31.1 0.0 copy-done
  31.1 5.2 fusion.3
  36.3 0.0 copy-start.1
  36.3 0.0 copy-start.4
  36.3 0.0 reduce-scatter.7.cloned.1.call-update
  36.4 0.0 reduce-scatter.5.cloned.1.call-start
  36.4 1.0 copy-done.1
  37.4 0.0 copy-done.4
  37.4 6.1 fusion.5
  43.5 0.0 reduce-scatter.5.cloned.1.call-update
  43.5 0.0 all-gather.3.cloned.1.call-start
  43.5 101.2 %reduce-scatter.7.cloned.1.call-done = f32[64,2816]{1,0:T(8,128)} async-done(((f32[512,2816]{1,0:T(8,128)}), f32[64,2816]{1,0:T(8,128)}) %reduce-scatter.7.cloned.1.call-update) | async-done | bytes 720912 | tf_op jit(solution)/shard_map/reduce_scatter | solution.py:22
  144.7 113.7 %reduce-scatter.5.cloned.1.call-done = f32[64,2816]{1,0:T(8,128)} async-done(((f32[512,2816]{1,0:T(8,128)}), f32[64,2816]{1,0:T(8,128)}) %reduce-scatter.5.cloned.1.call-update) | async-done | bytes 720912 | tf_op jit(solution)/shard_map/reduce_scatter | solution.py:21
  258.4 2.3 multiply_convert_fusion.2
  260.7 0.0 all-gather.3.cloned.1.call-update
  260.7 0.0 copy-start.2
  260.7 0.0 all-reduce.3.cloned.1.call-start
  260.8 56.7 %all-gather.3.cloned.1.call-done = bf16[512,2816]{1,0:T(8,128)(2,1)} async-done(((bf16[64,2816]{1,0:T(8,128)(2,1)}), bf16[512,2816]{1,0:T(8,128)(2,1)}) %all-gather.3.cloned.1.call-update) | async-done | bytes 2883600 | tf_op jit(solution)/shard_map/all_gather | solution.py:26
  317.5 5.3 fusion.9
  322.8 0.0 copy-start.3
  322.8 0.0 all-reduce.3.cloned.1.call-update
  322.8 0.0 reduce-scatter.11.cloned.1.call-start
  322.9 35.0 %all-reduce.3.cloned.1.call-done = f32[512,512]{1,0:T(8,128)} async-done(((f32[512,512]{1,0:T(8,128)}), f32[512,512]{1,0:T(8,128)}) %all-reduce.3.cloned.1.call-update) | async-done | bytes 1048592 | tf_op jit(solution)/shard_map/psum | solution.py:30
  357.9 1.4 multiply_reduce_fusion.2
  359.3 21.4 %psum.44 = f32[512]{0:T(512)S(1)} all-reduce(f32[512]{0:T(512)S(1)} %multiply_reduce_fusion.2), channel_id=1, replica_groups=mesh['ra'=8,'cb'=4] {'ra'}, use_global_device_ids=true, to_apply=%region_6.7 | all-reduce | flops 512 | bytes 4096 | tf_op jit(solution)/shard_map/psum | solution.py:51
  380.6 0.0 copy-done.2
  380.6 1.6 multiply_reduce_fusion.1
  382.2 17.1 %psum.45 = f32[512]{0:T(512)S(1)} all-reduce(f32[512]{0:T(512)S(1)} %multiply_reduce_fusion.1), channel_id=1, replica_groups=mesh['ra'=8,'cb'=4] {'ra'}, use_global_device_ids=true, to_apply=%region_8.9 | all-reduce | flops 512 | bytes 4096 | tf_op jit(solution)/shard_map/psum | solution.py:54
  399.3 0.0 copy-done.3
  399.4 6.4 fusion.7
  405.8 0.0 reduce-scatter.11.cloned.1.call-update
  405.8 0.0 reduce-scatter.9.cloned.1.call-start
  405.9 6.5 fusion.8
  412.4 0.0 reduce-scatter.9.cloned.1.call-update
  412.4 0.0 all-gather.5.cloned.1.call-start
  412.4 102.8 %reduce-scatter.11.cloned.1.call-done = f32[64,2816]{1,0:T(8,128)} async-done(((f32[512,2816]{1,0:T(8,128)}), f32[64,2816]{1,0:T(8,128)}) %reduce-scatter.11.cloned.1.call-update) | async-done | bytes 720912 | tf_op jit(solution)/shard_map/reduce_scatter | solution.py:22
  515.2 113.5 %reduce-scatter.9.cloned.1.call-done = f32[64,2816]{1,0:T(8,128)} async-done(((f32[512,2816]{1,0:T(8,128)}), f32[64,2816]{1,0:T(8,128)}) %reduce-scatter.9.cloned.1.call-update) | async-done | bytes 720912 | tf_op jit(solution)/shard_map/reduce_scatter | solution.py:21
  628.7 2.3 multiply_convert_fusion.1
  631.0 0.0 all-gather.5.cloned.1.call-update
  631.0 0.0 copy-start.5
  631.0 0.0 all-reduce.5.cloned.1.call-start
  631.0 56.7 %all-gather.5.cloned.1.call-done = bf16[512,2816]{1,0:T(8,128)(2,1)} async-done(((bf16[64,2816]{1,0:T(8,128)(2,1)}), bf16[512,2816]{1,0:T(8,128)(2,1)}) %all-gather.5.cloned.1.call-update) | async-done | bytes 2883600 | tf_op jit(solution)/shard_map/all_gather | solution.py:26
  687.8 5.3 fusion.10
  693.1 0.0 all-reduce.5.cloned.1.call-update
  693.1 35.1 %all-reduce.5.cloned.1.call-done = f32[512,512]{1,0:T(8,128)} async-done(((f32[512,512]{1,0:T(8,128)}), f32[512,512]{1,0:T(8,128)}) %all-reduce.5.cloned.1.call-update) | async-done | bytes 1048592 | tf_op jit(solution)/shard_map/psum | solution.py:30
  728.2 1.4 multiply_reduce_fusion
  729.5 21.4 %psum.47 = f32[512]{0:T(512)S(1)} all-reduce(f32[512]{0:T(512)S(1)} %multiply_reduce_fusion), channel_id=1, replica_groups=mesh['ra'=8,'cb'=4] {'ra'}, use_global_device_ids=true, to_apply=%region_13.14 | all-reduce | flops 512 | bytes 4096 | tf_op jit(solution)/shard_map/psum | solution.py:58
  750.9 0.0 copy-done.5
  750.9 2.7 add_convert_fusion
  (4 shorter events, 0.0 us)
Async XLA Ops:
  6.5 24.5 %copy-start = (bf16[512,2816]{1,0:T(8,128)(2,1)S(1)}, bf16[512,2816]{1,0:T(8,128)(2,1)}, u32[]{:S(2)}) copy-start(bf16[512,2816]{1,0:T(8,128)(2,1)} %param.14) | copy-start | bytes 8650756
  6.5 138.2 %reduce-scatter.7.cloned.1.call-start = ((), (), s32[]{:S(2)}) async-start(), calls=%async_computation.5 | async-start | bytes 6488064 | tf_op jit(solution)/shard_map/reduce_scatter | solution.py:22
  36.3 1.0 copy-start.1
  36.3 1.0 copy-start.4
  36.4 222.1 %reduce-scatter.5.cloned.1.call-start = ((), (), s32[]{:S(2)}) async-start(), calls=%async_computation.4 | async-start | bytes 6488064 | tf_op jit(solution)/shard_map/reduce_scatter | solution.py:21
  43.5 274.0 %all-gather.3.cloned.1.call-start = ((), (), s32[]{:S(2)}) async-start(), calls=%async_computation.6 | async-start | bytes 3244032 | tf_op jit(solution)/shard_map/all_gather | solution.py:26
  260.7 119.9 %copy-start.2 = (f32[512]{0:T(512)S(1)}, f32[512]{0:T(512)}, u32[]{:S(2)}) copy-start(f32[512]{0:T(512)} %param.16) | copy-start | bytes 6148
  260.7 97.2 %all-reduce.3.cloned.1.call-start = ((), (), s32[]{:S(2)}) async-start(), calls=%async_computation.7 | async-start | bytes 2097152 | tf_op jit(solution)/shard_map/psum | solution.py:30
  322.8 76.6 %copy-start.3 = (f32[512]{0:T(512)S(1)}, f32[512]{0:T(512)}, u32[]{:S(2)}) copy-start(f32[512]{0:T(512)} %param.17) | copy-start | bytes 6148
  322.8 192.4 %reduce-scatter.11.cloned.1.call-start = ((), (), s32[]{:S(2)}) async-start(), calls=%async_computation.9 | async-start | bytes 6488064 | tf_op jit(solution)/shard_map/reduce_scatter | solution.py:22
  405.8 222.9 %reduce-scatter.9.cloned.1.call-start = ((), (), s32[]{:S(2)}) async-start(), calls=%async_computation.8 | async-start | bytes 6488064 | tf_op jit(solution)/shard_map/reduce_scatter | solution.py:21
  412.4 275.4 %all-gather.5.cloned.1.call-start = ((), (), s32[]{:S(2)}) async-start(), calls=%async_computation.10 | async-start | bytes 3244032 | tf_op jit(solution)/shard_map/all_gather | solution.py:26
  631.0 119.9 %copy-start.5 = (f32[512]{0:T(512)S(1)}, f32[512]{0:T(512)}, u32[]{:S(2)}) copy-start(f32[512]{0:T(512)} %param.21) | copy-start | bytes 6148
  631.0 97.2 %all-reduce.5.cloned.1.call-start = ((), (), s32[]{:S(2)}) async-start(), calls=%async_computation.11 | async-start | bytes 2097152 | tf_op jit(solution)/shard_map/psum | solution.py:30
Sparse Core Ops, SparseCore 0:
  36.5 108.2 reduce-scatter.6
  148.4 109.9 reduce-scatter.4
  260.8 56.6 all-gather.2
  322.9 34.8 all-reduce.2
  405.9 109.2 reduce-scatter.10
  518.7 109.9 reduce-scatter.8
  631.1 56.6 all-gather.4
  693.2 34.8 all-reduce.4
where the time goes:
time: 761 us; the launch traced here: 760 us
  waiting for transfers between devices  615 us (81%)
  blocking collectives  83 us (11%)
  matrix products  34.9 us (5%)
  between operations  13.5 us (2%)
  other arithmetic  12.9 us (2%)
    reduce_scatter x2, waiting for transfers between devices, branch_value(): lax.psum_scatter(gate_value, 'ra', scatter_dimension=0, tiled=True)  227 us
    reduce_scatter x2, waiting for transfers between devices, branch_value(): lax.psum_scatter(up_value, 'ra', scatter_dimension=0, tiled=True)  204 us
    all_gather x2, waiting for transfers between devices, branch_value(): lax.all_gather(hidden, 'ra', axis=0, tiled=True)  113 us
    psum x2, waiting for transfers between devices, branch_value(): return lax.psum(partial_out, 'cb')  70.1 us
    psum x1, blocking collectives, body(): input_total = lax.psum(jnp.sum(resid * resid, axis=1), 'ra')  23.2 us
    psum x1, blocking collectives, body(): first_total = lax.psum(jnp.sum(branch_first * branch_first, axis=1), 'ra')  21.4 us
    psum x1, blocking collectives, body(): lax.psum(jnp.sum(branch_second * branch_second, axis=1), 'ra')  21.4 us
    psum x1, blocking collectives, body(): middle_total = lax.psum(jnp.sum(middle * middle, axis=1), 'ra')  17.1 us
  transfers between devices with their start and end apart: 8, of which 8 were waited for; matrix products, arithmetic and copies ran while one was open for 2% of the time, Pallas kernels for 0%

commit v1 on v0

v1 whole, which is shorter than its diff:
```python
import functools

import jax
import jax.numpy as jnp
from jax import lax
from jax.experimental import pallas as pl
from jax.experimental.pallas import tpu as pltpu
from jax.sharding import PartitionSpec as P

EPS = 1e-06
MESH = pl.DeviceIdType.MESH
F32 = jnp.float32
BF16 = jnp.bfloat16


def log2(n):
    return n.bit_length() - 1


def bits_of(index, count):
    return [lax.rem(index // (1 << b), 2) for b in range(count)]


def spread(col, lanes):
    return jnp.broadcast_to(col, (col.shape[0], 128)).T[0:8]


def column(row):
    return jnp.broadcast_to(row[0:1], (128, row.shape[1])).T


def half_step(
    first, n, nc, width, *refs
):
    k, kc = log2(n), log2(nc)
    (h_ref, resid_ref, ss_ref, post_ref, pre_ref, gate_hbm, up_hbm, down_hbm), refs = refs[:8], refs[8:]
    if first:
        (h_out, mid_out, ss_out), refs = refs[:3], refs[3:]
    else:
        (y_out,), refs = refs[:1], refs[1:]
    (gate_v, up_v, down_v, acc, hid, branch, scale, ss_slots, br_slots, br_send, ag, ss_all), refs = refs[:12], refs[12:]
    snd, refs = refs[:k], refs[k:]
    rcv, refs = refs[:k], refs[k:]
    csnd, refs = refs[:kc], refs[kc:]
    crcv, refs = refs[:kc], refs[kc:]
    (w_sem, rs_s, rs_r, ag_s, ag_r, c_s, c_r, ss_s, ss_r, br_s, br_r, cg_s, cg_r, cs_s, cs_r) = refs

    tokens, depth = h_ref.shape
    chunks, _, cw = gate_v.shape
    me, col = lax.axis_index("ra"), lax.axis_index("cb")
    eb, xb = bits_of(me, k), bits_of(col, kc)
    partners = [me + (1 - 2 * eb[b]) * (1 << b) for b in range(k)]
    cpartners = [col + (1 - 2 * xb[b]) * (1 << b) for b in range(kc)]
    crows = tokens // nc

    def weights(c):
        cols = pl.ds(pl.multiple_of(c * cw, 128), cw)
        return [
            pltpu.make_async_copy(gate_hbm.at[:, cols], gate_v.at[c], w_sem.at[0, c]),
            pltpu.make_async_copy(up_hbm.at[:, cols], up_v.at[c], w_sem.at[1, c]),
            pltpu.make_async_copy(down_hbm.at[cols, :], down_v.at[c], w_sem.at[2, c]),
        ]

    @pl.loop(0, chunks)
    def _(c):
        for copy in weights(c):
            copy.start()

    barrier = pltpu.get_barrier_semaphore()

    def xor(index, bits, off):
        out = index
        for b, bit in enumerate(bits):
            if (off >> b) & 1:
                out = out + (1 - 2 * bit) * (1 << b)
        return out

    for off in range(1, n):
        pl.semaphore_signal(barrier, inc=1, device_id={"ra": xor(me, eb, off)}, device_id_type=MESH)
    for off in range(1, nc):
        pl.semaphore_signal(barrier, inc=1, device_id={"cb": xor(col, xb, off)}, device_id_type=MESH)
    pl.semaphore_wait(barrier, n - 1 + nc - 1)

    def remote(src, dst, s, r, **where):
        return pltpu.make_async_remote_copy(
            src_ref=src, dst_ref=dst, send_sem=s, recv_sem=r, device_id=where, device_id_type=MESH
        )

    def ss_copy(off):
        return remote(ss_ref, ss_slots.at[off - 1], ss_s.at[off - 1], ss_r.at[off - 1], ra=xor(me, eb, off))

    for off in range(1, n):
        ss_copy(off).start()

    def plan(c):
        swap = jnp.where(lax.rem(c, 4) == 1, 1, 0)
        bits, to = list(eb), list(partners)
        if k > 1:
            bits[0], bits[1] = eb[0] + swap * (eb[1] - eb[0]), eb[1] + swap * (eb[0] - eb[1])
            to[0] = partners[0] + swap * (partners[1] - partners[0])
            to[1] = partners[1] + swap * (partners[0] - partners[1])
        return bits, to

    def rows_at(base, size):
        return pl.ds(pl.multiple_of(base, size), size)

    def rs_copy(c, s, to):
        return remote(snd[s].at[c], rcv[s].at[c], rs_s.at[s, c], rs_r.at[s, c], ra=to[s])

    def ag_copy(c, s, bits, to):
        size = tokens >> (s + 1)
        base = sum(bits[i] * (tokens >> (i + 1)) for i in range(s + 1))
        part = hid.at[c, rows_at(base, size), :]
        return remote(part, part, ag_s.at[s, c], ag_r.at[s, c], ra=to[s])

    branch[...] = jnp.zeros_like(branch)

    def tick(t, carry):
        @pl.when(t < chunks)
        def _():
            c = t
            bits, to = plan(c)
            gate_copy, up_copy, _ = weights(c)
            gate_copy.wait()
            up_copy.wait()
            half = tokens // 2
            theirs = h_ref[rows_at((1 - bits[0]) * half, half), :]
            snd[0][c, :, :cw] = jnp.dot(theirs, gate_v[c], preferred_element_type=F32).astype(BF16)
            snd[0][c, :, cw:] = jnp.dot(theirs, up_v[c], preferred_element_type=F32).astype(BF16)
            rs_copy(c, 0, to).start()
            mine = h_ref[rows_at(bits[0] * half, half), :]
            acc[c, :, :cw] = jnp.dot(mine, gate_v[c], preferred_element_type=F32)
            acc[c, :, cw:] = jnp.dot(mine, up_v[c], preferred_element_type=F32)

        for s in range(1, k):
            @pl.when((t >= s) & (t < chunks + s))
            def _():
                c = t - s
                bits, to = plan(c)
                rs_copy(c, s - 1, to).wait()
                size = tokens >> (s + 1)
                base = sum(bits[i] * (tokens >> (i + 1)) for i in range(1, s))
                out = (1 - bits[s]) * size
                snd[s][c] = (
                    acc[c, rows_at(base + out, size), :] + rcv[s - 1][c, rows_at(out, size), :].astype(F32)
                ).astype(BF16)
                rs_copy(c, s, to).start()
                keep = bits[s] * size
                acc[c, rows_at(base + keep, size), :] += rcv[s - 1][c, rows_at(keep, size), :].astype(F32)

        @pl.when(t == k)
        def _():
            for off in range(1, n):
                ss_copy(off).wait()
            total = ss_ref[...]
            for off in range(1, n):
                total = total + ss_slots[off - 1]
            for b in range(nc):
                scale[b * crows : (b + 1) * crows, :] = column(lax.rsqrt(total[b] / width + EPS))

        @pl.when((t >= k) & (t < chunks + k))
        def _():
            c = t - k
            bits, to = plan(c)
            rs_copy(c, k - 1, to).wait()
            size = tokens >> k
            base = sum(bits[i] * (tokens >> (i + 1)) for i in range(1, k))
            value = acc[c, rows_at(base, size), :] + rcv[k - 1][c].astype(F32)
            rows = rows_at(base + bits[0] * (tokens // 2), size)
            factor = scale[rows, 0:1]
            g, u = value[:, :cw] * factor, value[:, cw:] * factor
            hid[c, rows, :] = (g / (1.0 + jnp.exp(-g)) * u).astype(BF16)
            ag_copy(c, k - 1, bits, to).start()

        for s in range(k - 1, 0, -1):
            lag = 2 * k - s
            @pl.when((t >= lag) & (t < chunks + lag))
            def _():
                c = t - lag
                bits, to = plan(c)
                ag_copy(c, s, bits, to).wait()
                ag_copy(c, s - 1, bits, to).start()

        @pl.when(t >= 2 * k)
        def _():
            c = t - 2 * k
            bits, to = plan(c)
            ag_copy(c, 0, bits, to).wait()
            weights(c)[2].wait()
            branch[...] += jnp.dot(hid[c], down_v[c], preferred_element_type=F32)

        return carry

    lax.fori_loop(0, chunks + 2 * k, tick, 0)

    def c_copy(s):
        return remote(csnd[s], crcv[s], c_s.at[s], c_r.at[s], cb=cpartners[s])

    base = 0
    for s in range(kc):
        size = tokens >> (s + 1)
        out, keep = (1 - xb[s]) * size, xb[s] * size
        mine = branch[rows_at(base + out, size), :]
        if s:
            mine = mine + crcv[s - 1][rows_at(out, size), :].astype(F32)
        csnd[s][...] = mine.astype(csnd[s].dtype)
        c_copy(s).start()
        if s:
            branch[rows_at(base + keep, size), :] += crcv[s - 1][rows_at(keep, size), :].astype(F32)
        c_copy(s).wait()
        base = base + keep
    own = rows_at(base, crows)
    total = branch[own, :] + crcv[kc - 1][...].astype(F32)

    br_send[...] = spread(jnp.sum(total * total, axis=1, keepdims=True), crows)

    def br_copy(off):
        return remote(br_send, br_slots.at[off - 1], br_s.at[off - 1], br_r.at[off - 1], ra=xor(me, eb, off))

    for off in range(1, n):
        br_copy(off).start()
    squares = br_send[...]
    for off in range(1, n):
        br_copy(off).wait()
        squares = squares + br_slots[off - 1]
    factor = column(0.5 * lax.rsqrt(squares / width + EPS))[:, 0:1]
    resid = resid_ref[own, :].astype(F32) if first else resid_ref[...]
    middle = resid + factor * total * post_ref[...]
    if first:
        ag[own, :] = (middle * pre_ref[...]).astype(BF16)
        mid_out[...] = middle
    else:
        ag[own, :] = middle.astype(BF16)

    bases = [0]
    for s in range(kc):
        bases.append(bases[-1] + xb[s] * (tokens >> (s + 1)))

    def cg_copy(s):
        part = ag.at[rows_at(bases[s + 1], tokens >> (s + 1)), :]
        return remote(part, part, cg_s.at[s], cg_r.at[s], cb=cpartners[s])

    cg_copy(kc - 1).start()
    if first:
        block = sum(xb[s] * (nc >> (s + 1)) for s in range(kc))
        ss_all[block] = spread(jnp.sum(middle * middle, axis=1, keepdims=True), crows)

        def cs_copy(off):
            part = ss_all.at[block]
            return remote(part, part, cs_s.at[off - 1], cs_r.at[off - 1], cb=xor(col, xb, off))

        for off in range(1, nc):
            cs_copy(off).start()
    for s in range(kc - 1, -1, -1):
        cg_copy(s).wait()
        if s:
            cg_copy(s - 1).start()
    if first:
        for off in range(1, nc):
            cs_copy(off).wait()
        ss_out[...] = ss_all[...]
        h_out[...] = ag[...]
    else:
        y_out[...] = ag[...]


def run(first, n, nc, width, h, resid, ss, post, pre, gate, up, down):
    tokens, depth = h.shape
    hidden = gate.shape[1]
    cw = 256 if hidden % 256 == 0 else 128
    chunks = hidden // cw
    k, kc, crows = log2(n), log2(nc), tokens // nc
    vmem = pl.BlockSpec(memory_space=pltpu.VMEM)
    hbm = pl.BlockSpec(memory_space=pl.ANY)
    dma = pltpu.SemaphoreType.DMA
    if first:
        out = [
            jax.ShapeDtypeStruct((tokens, depth), BF16),
            jax.ShapeDtypeStruct((crows, depth), F32),
            jax.ShapeDtypeStruct((nc, 8, crows), F32),
        ]
    else:
        out = [jax.ShapeDtypeStruct((tokens, depth), BF16)]
    scratch = [
        pltpu.VMEM((chunks, depth, cw), BF16),
        pltpu.VMEM((chunks, depth, cw), BF16),
        pltpu.VMEM((chunks, cw, depth), BF16),
        pltpu.VMEM((chunks, tokens // 2, 2 * cw), F32),
        pltpu.VMEM((chunks, tokens, cw), BF16),
        pltpu.VMEM((tokens, depth), F32),
        pltpu.VMEM((tokens, 128), F32),
        pltpu.VMEM((n - 1, nc, 8, crows), F32),
        pltpu.VMEM((n - 1, 8, crows), F32),
        pltpu.VMEM((8, crows), F32),
        pltpu.VMEM((tokens, depth), BF16),
        pltpu.VMEM((nc, 8, crows), F32),
    ]
    scratch += [pltpu.VMEM((chunks, tokens >> (s + 1), 2 * cw), BF16) for s in range(k)] * 2
    scratch += [pltpu.VMEM((tokens >> (s + 1), depth), BF16 if s else F32) for s in range(kc)] * 2
    scratch += [dma((3, chunks))] + [dma((k, chunks))] * 4 + [dma((kc,))] * 2
    scratch += [dma((n - 1,))] * 4 + [dma((kc,))] * 2 + [dma((nc - 1,))] * 2
    return pl.pallas_call(
        functools.partial(half_step, first, n, nc, width),
        out_shape=out,
        in_specs=[vmem] * 5 + [hbm] * 3,
        out_specs=[vmem] * len(out),
        scratch_shapes=scratch,
        compiler_params=pltpu.CompilerParams(
            collective_id=0 if first else 1, has_side_effects=True, vmem_limit_bytes=60 * 1024 * 1024
        ),
        name="first" if first else "second",
    )(h, resid, ss, post, pre, gate, up, down)


def solution(mesh):
    n, nc = mesh.shape["ra"], mesh.shape["cb"]

    def body(tokens, pre1, gate1, up1, down1, post1, pre2, gate2, up2, down2, post2):
        count, depth = tokens.shape
        width = depth * n
        resid = tokens.astype(F32)
        squares = jnp.sum(resid * resid, axis=1).reshape(nc, 1, count // nc)
        ss = jnp.broadcast_to(squares, (nc, 8, count // nc))
        h = (resid * pre1[None, :]).astype(BF16)
        row = lambda gain: gain.reshape(1, depth)
        h2, mid, ss2 = run(True, n, nc, width, h, tokens, ss, row(post1), row(pre2), gate1, up1, down1)
        (out,) = run(False, n, nc, width, h2, mid, ss2, row(post2), row(pre2), gate2, up2, down2)
        return out

    in_specs = (
        P(None, "ra"), P("ra"), P("ra", "cb"), P("ra", "cb"), P("cb", "ra"), P("ra"),
        P("ra"), P("ra", "cb"), P("ra", "cb"), P("cb", "ra"), P("ra"),
    )
    return jax.shard_map(body, mesh=mesh, in_specs=in_specs, out_specs=P(None, "ra"), check_vma=False)
```

time: 761 us -> 254 us (0.33)
  waiting for transfers between devices: 615 us -> 0 us
  Pallas kernels: 0 us -> 249 us
  blocking collectives: 83 us -> 0 us
  matrix products: 34.9 us -> 0 us
  between operations: 13.5 us -> 0.02 us
  other arithmetic: 12.9 us -> 1.98 us
    reduce_scatter x4 -> x0, waiting for transfers between devices: 431 us -> none  [the longest x2 227 us: branch_value(): lax.psum_scatter(gate_value, 'ra', scatter_dimension=0, tiled=True)]
    pallas_call x0 -> x2, Pallas kernels: none -> 249 us  [run(): pl.pallas_call(functools.partial(half_step, first, n, nc, width), out_sha...]
    all_gather x2 -> x0, waiting for transfers between devices: 113 us -> none  [branch_value(): lax.all_gather(hidden, 'ra', axis=0, tiled=True)]
    psum x4 -> x0, blocking collectives: 83 us -> none  [the longest x1 23.2 us: body(): input_total = lax.psum(jnp.sum(resid * resid, axis=1), 'ra')]
    psum x2 -> x0, waiting for transfers between devices: 70.1 us -> none  [branch_value(): return lax.psum(partial_out, 'cb')]
    dot_general x6 -> x0, matrix products: 34.9 us -> none  [the longest x2 12.6 us: branch_value(): jnp.dot(normed, gate_weight, preferred_element_type=jnp.float32)]
  transfers between devices with their start and end apart: 8 -> 0, of which waited for: 8 -> 0; matrix products, arithmetic and copies ran while one was open for 2% -> 0% of each run, Pallas kernels for 0% -> 0%
where the time goes in v1:
time: 254 us
  Pallas kernels  249 us (98%)
    pallas_call x2, Pallas kernels, run(): pl.pallas_call(functools.partial(half_step, first, n, nc, width), out_sha...  249 us

profile of v1, /device:TPU:0, one launch (start us, length us, event | category | flops | bytes accessed | tf_op | source)
XLA Modules:
  0.0 253.9 jit_solution(13429112706994295951)
XLA Ops:
  0.0 2.0 fusion.1
  2.0 0.6 broadcast_in_dim.9.refs_2_
  2.6 125.7 %first.1 = (bf16[512,512]{1,0:T(8,128)(2,1)}, f32[128,512]{1,0:T(8,128)}, f32[4,8,128]{2,1,0:T(8,128)}) custom-call(bf16[512,512]{1,0:T(8,128)(2,1)} %get-tuple-element.12.refs_0_, bf16[512,512]{1,0:T(8,128)(2,1)} %refs_1_.1, f32[4,8,128]{2,1,0:T(8,128)} %broadcast_in_dim.9.refs_2_, f32[1,512]{1,0:T(1,128)} %bitcast.7, f32[1,512]{1,0:T(1,128)} %bitcast.4, ...), custom_call_target="tpu_custom_call" | custom-call | tf_op jit(solution)/shard_map/first/pallas_call | solution.py:302
  128.3 123.7 %second.1 = bf16[512,512]{1,0:T(8,128)(2,1)} custom-call(bf16[512,512]{1,0:T(8,128)(2,1)} %get-tuple-element.8.refs_0_, f32[128,512]{1,0:T(8,128)} %get-tuple-element.9.refs_1_, f32[4,8,128]{2,1,0:T(8,128)} %get-tuple-element.10.refs_2_, f32[1,512]{1,0:T(1,128)} %bitcast.8, f32[1,512]{1,0:T(1,128)} %bitcast.5, bf16[512,2816]{1,0:T(8,128)(2,1)} %refs_5_.3, ...), custom_call_target="tpu_custom_call" | custom-call | tf_op jit(solution)/shard_map/second/pallas_call | solution.py:302
  252.0 1.9 copy.13

commit v2 on v1

--- a/solution.py
+++ b/solution.py
@@ -38,7 +38,7 @@
         (h_out, mid_out, ss_out), refs = refs[:3], refs[3:]
     else:
         (y_out,), refs = refs[:1], refs[1:]
-    (gate_v, up_v, down_v, acc, hid, branch, scale, ss_slots, br_slots, br_send, ag, ss_all), refs = refs[:12], refs[12:]
+    (both_v, down_v, acc, hid, branch, scale, ss_slots, br_slots, br_send, ag, ss_all), refs = refs[:11], refs[11:]
     snd, refs = refs[:k], refs[k:]
     rcv, refs = refs[:k], refs[k:]
     csnd, refs = refs[:kc], refs[kc:]
@@ -46,7 +46,7 @@
     (w_sem, rs_s, rs_r, ag_s, ag_r, c_s, c_r, ss_s, ss_r, br_s, br_r, cg_s, cg_r, cs_s, cs_r) = refs
 
     tokens, depth = h_ref.shape
-    chunks, _, cw = gate_v.shape
+    chunks, cw, _ = down_v.shape
     me, col = lax.axis_index("ra"), lax.axis_index("cb")
     eb, xb = bits_of(me, k), bits_of(col, kc)
     partners = [me + (1 - 2 * eb[b]) * (1 << b) for b in range(k)]
@@ -56,8 +56,8 @@
     def weights(c):
         cols = pl.ds(pl.multiple_of(c * cw, 128), cw)
         return [
-            pltpu.make_async_copy(gate_hbm.at[:, cols], gate_v.at[c], w_sem.at[0, c]),
-            pltpu.make_async_copy(up_hbm.at[:, cols], up_v.at[c], w_sem.at[1, c]),
+            pltpu.make_async_copy(gate_hbm.at[:, cols], both_v.at[c, :, pl.ds(0, cw)], w_sem.at[0, c]),
+            pltpu.make_async_copy(up_hbm.at[:, cols], both_v.at[c, :, pl.ds(cw, cw)], w_sem.at[1, c]),
             pltpu.make_async_copy(down_hbm.at[cols, :], down_v.at[c], w_sem.at[2, c]),
         ]
 
@@ -93,7 +93,7 @@
         ss_copy(off).start()
 
     def plan(c):
-        swap = jnp.where(lax.rem(c, 4) == 1, 1, 0)
+        swap = jnp.where(lax.rem(c, 3) == 1, 1, 0)
         bits, to = list(eb), list(partners)
         if k > 1:
             bits[0], bits[1] = eb[0] + swap * (eb[1] - eb[0]), eb[1] + swap * (eb[0] - eb[1])
@@ -114,6 +114,8 @@
         return remote(part, part, ag_s.at[s, c], ag_r.at[s, c], ra=to[s])
 
     branch[...] = jnp.zeros_like(branch)
+
+    lags = [2 * i for i in range(2 * k + 1)]
 
     def tick(t, carry):
         @pl.when(t < chunks)
@@ -125,17 +127,16 @@
             up_copy.wait()
             half = tokens // 2
             theirs = h_ref[rows_at((1 - bits[0]) * half, half), :]
-            snd[0][c, :, :cw] = jnp.dot(theirs, gate_v[c], preferred_element_type=F32).astype(BF16)
-            snd[0][c, :, cw:] = jnp.dot(theirs, up_v[c], preferred_element_type=F32).astype(BF16)
+            snd[0][c] = jnp.dot(theirs, both_v[c], preferred_element_type=F32).astype(BF16)
             rs_copy(c, 0, to).start()
             mine = h_ref[rows_at(bits[0] * half, half), :]
-            acc[c, :, :cw] = jnp.dot(mine, gate_v[c], preferred_element_type=F32)
-            acc[c, :, cw:] = jnp.dot(mine, up_v[c], preferred_element_type=F32)
+            acc[c] = jnp.dot(mine, both_v[c], preferred_element_type=F32)
 
         for s in range(1, k):
-            @pl.when((t >= s) & (t < chunks + s))
+            rs_lag = lags[s]
+            @pl.when((t >= rs_lag) & (t < chunks + rs_lag))
             def _():
-                c = t - s
+                c = t - rs_lag
                 bits, to = plan(c)
                 rs_copy(c, s - 1, to).wait()
                 size = tokens >> (s + 1)
@@ -148,7 +149,7 @@
                 keep = bits[s] * size
                 acc[c, rows_at(base + keep, size), :] += rcv[s - 1][c, rows_at(keep, size), :].astype(F32)
 
-        @pl.when(t == k)
+        @pl.when(t == lags[k])
         def _():
             for off in range(1, n):
                 ss_copy(off).wait()
@@ -158,9 +159,9 @@
             for b in range(nc):
                 scale[b * crows : (b + 1) * crows, :] = column(lax.rsqrt(total[b] / width + EPS))
 
-        @pl.when((t >= k) & (t < chunks + k))
+        @pl.when((t >= lags[k]) & (t < chunks + lags[k]))
         def _():
-            c = t - k
+            c = t - lags[k]
             bits, to = plan(c)
             rs_copy(c, k - 1, to).wait()
             size = tokens >> k
@@ -173,7 +174,7 @@
             ag_copy(c, k - 1, bits, to).start()
 
         for s in range(k - 1, 0, -1):
-            lag = 2 * k - s
+            lag = lags[2 * k - s]
             @pl.when((t >= lag) & (t < chunks + lag))
             def _():
                 c = t - lag
@@ -181,9 +182,9 @@
                 ag_copy(c, s, bits, to).wait()
                 ag_copy(c, s - 1, bits, to).start()
 
-        @pl.when(t >= 2 * k)
+        @pl.when(t >= lags[2 * k])
         def _():
-            c = t - 2 * k
+            c = t - lags[2 * k]
             bits, to = plan(c)
             ag_copy(c, 0, bits, to).wait()
             weights(c)[2].wait()
@@ -191,7 +192,7 @@
 
         return carry
 
-    lax.fori_loop(0, chunks + 2 * k, tick, 0)
+    lax.fori_loop(0, chunks + lags[2 * k], tick, 0)
 
     def c_copy(s):
         return remote(csnd[s], crcv[s], c_s.at[s], c_r.at[s], cb=cpartners[s])
@@ -282,8 +283,7 @@
     else:
         out = [jax.ShapeDtypeStruct((tokens, depth), BF16)]
     scratch = [
-        pltpu.VMEM((chunks, depth, cw), BF16),
-        pltpu.VMEM((chunks, depth, cw), BF16),
+        pltpu.VMEM((chunks, depth, 2 * cw), BF16),
         pltpu.VMEM((chunks, cw, depth), BF16),
         pltpu.VMEM((chunks, tokens // 2, 2 * cw), F32),
         pltpu.VMEM((chunks, tokens, cw), BF16),

time: 254 us -> 241 us (0.949)
  Pallas kernels: 249 us -> 236 us
    pallas_call x2, Pallas kernels: 249 us -> 236 us  [run(): pl.pallas_call(functools.partial(half_step, first, n, nc, width), out_sha...]
where the time goes in v2:
time: 241 us; the launch traced here: 240 us
  Pallas kernels  236 us (98%)
  local copies, waits for them, and re-layouts  2.47 us (1%)
    pallas_call x2, Pallas kernels, run(): pl.pallas_call(functools.partial(half_step, first, n, nc, width), out_sha...  236 us

profile of v2, /device:TPU:0, one launch (start us, length us, event | category | flops | bytes accessed | tf_op | source)
XLA Modules:
  0.0 240.4 jit_solution(5738517245608402508)
XLA Ops:
  0.0 2.0 fusion.1
  2.0 0.6 broadcast_in_dim.9.refs_2_
  2.6 119.2 %first.1 = (bf16[512,512]{1,0:T(8,128)(2,1)}, f32[128,512]{1,0:T(8,128)}, f32[4,8,128]{2,1,0:T(8,128)}) custom-call(bf16[512,512]{1,0:T(8,128)(2,1)} %get-tuple-element.12.refs_0_, bf16[512,512]{1,0:T(8,128)(2,1)} %refs_1_.1, f32[4,8,128]{2,1,0:T(8,128)} %broadcast_in_dim.9.refs_2_, f32[1,512]{1,0:T(1,128)} %bitcast.7, f32[1,512]{1,0:T(1,128)} %bitcast.4, ...), custom_call_target="tpu_custom_call" | custom-call | tf_op jit(solution)/shard_map/first/pallas_call | solution.py:302
  121.8 116.8 %second.1 = bf16[512,512]{1,0:T(8,128)(2,1)} custom-call(bf16[512,512]{1,0:T(8,128)(2,1)} %get-tuple-element.8.refs_0_, f32[128,512]{1,0:T(8,128)} %get-tuple-element.9.refs_1_, f32[4,8,128]{2,1,0:T(8,128)} %get-tuple-element.10.refs_2_, f32[1,512]{1,0:T(1,128)} %bitcast.8, f32[1,512]{1,0:T(1,128)} %bitcast.5, bf16[512,2816]{1,0:T(8,128)(2,1)} %refs_5_.3, ...), custom_call_target="tpu_custom_call" | custom-call | tf_op jit(solution)/shard_map/second/pallas_call | solution.py:302
  238.6 1.9 copy.13
